TPU v7x, 32 devices: a whole 2x2x4 slice. The times are simulated.
32 devices in a mesh: kv: 8 (over z, y), tp: 4 (over x, core).
Axes of the slice: x: 2, y: 2, z: 4, core: 2. Of those that a mesh axis runs over, the one named last changes fastest.
Arguments:
- queries: bfloat16 [2, 3072, 1024], P(None, 'kv', 'tp'), may hold values from -112 to 112
- key_states: bfloat16 [2, 3072, 256], P(None, 'kv', 'tp'), may hold values from -4 to 4
- value_states: bfloat16 [2, 3072, 256], P(None, 'kv', 'tp'), may hold values from -6 to 6
- cotangent: bfloat16 [2, 3072, 1024], P(None, 'kv', 'tp'), may hold values from -6 to 6
- gate_logits: float32 [2, 3072, 16], P(None, 'kv', 'tp'), may hold values from -6 to 6
- layer_input: bfloat16 [2, 3072, 4096], P(None, ('kv', 'tp')), may hold values from -6 to 6
- chosen: int32 [2, 48, 4, 16], P(None, 'kv', 'tp'), may hold values from 0 to 47, as said below
Outputs:
- query_grad: bfloat16 [2, 3072, 1024], P(None, 'kv', 'tp')
- key_grad: bfloat16 [2, 3072, 256], P(None, 'kv', 'tp')
- value_grad: bfloat16 [2, 3072, 256], P(None, 'kv', 'tp')
- value_weight_grad: float32 [4096, 256], P(('kv', 'tp'))
Inputs may be any that keep to these rules, and one draw needn't show every extreme that they name: `chosen`: for each sequence, query block b and key head, the 16 entries are distinct blocks; they include b itself and block 0; blocks after b hold only keys after all of the block's queries. Taking the 6 query blocks of one index of kv together (aligned), one sequence and one key head, at most 2 distinct blocks held by any one earlier index of kv are named, and some index reaches 2.
All inputs are finite; a program needn't handle non-finite values.
Results may differ from a plain program's by a relative error of at most 0.0058.
Values may be sent and summed in bfloat16 or wider, within the bound.
No kernel may reach another device: no remote copies, remote signals or barrier semaphores. Data moves between devices by JAX's collectives and lax.ppermute only.
A program may use at most 128 MiB of HBM per device.

v0:
```python
import jax
import jax.numpy as jnp
from jax import lax
from jax.sharding import PartitionSpec as P

BLK = 64
MOST = 2


def on_device(queries, key_states, value_states, cotangent, gate_logits, layer_input, chosen):
    seq_count, tok_rows, row_width = queries.shape
    head_dim = key_states.shape[2]
    head_count = row_width // head_dim
    block_len = BLK
    blocks_dev = tok_rows // block_len
    pick_count = chosen.shape[3]
    devices = lax.axis_size("kv")
    own_index = lax.axis_index("kv")
    score_scale = head_dim ** (-0.5)
    all_keys, all_values = (
        lax.all_gather(key_states, "kv", axis=1, tiled=True),
        lax.all_gather(value_states, "kv", axis=1, tiled=True),
    )
    total_blocks = all_keys.shape[1] // block_len
    key_blocks = all_keys.reshape(seq_count, total_blocks, block_len, head_dim)
    value_blocks = all_values.reshape(seq_count, total_blocks, block_len, head_dim)
    chosen_ids = chosen[:, :, 0, :]
    seq_ids = jnp.arange(seq_count, dtype=jnp.int32)[:, None, None]
    picked_keys = key_blocks[seq_ids, chosen_ids]
    picked_values = value_blocks[seq_ids, chosen_ids]
    query_rows = queries.reshape(seq_count, blocks_dev, block_len, head_count, head_dim)
    scores = (
        jnp.einsum(
            "sbqhd,sbknd->sbhqkn", query_rows, picked_keys, preferred_element_type=jnp.float32
        )
        * score_scale
    )
    local_block = own_index * blocks_dev + jnp.arange(blocks_dev, dtype=jnp.int32)
    query_pos = local_block[:, None] * block_len + jnp.arange(block_len, dtype=jnp.int32)[None, :]
    key_pos = chosen_ids[..., None] * block_len + jnp.arange(block_len, dtype=jnp.int32)
    allowed = key_pos[:, :, None, None, :, :] <= query_pos[None, :, None, :, None, None]
    scores = jnp.where(allowed, scores, -jnp.inf)
    row_max = jnp.max(scores, axis=(4, 5), keepdims=True)
    exp_terms = jnp.exp(scores - row_max)
    weights = exp_terms / jnp.sum(exp_terms, axis=(4, 5), keepdims=True)
    weights_bf = weights.astype(jnp.bfloat16)
    branch_out = jnp.einsum(
        "sbhqkn,sbknd->sbqhd", weights_bf, picked_values, preferred_element_type=jnp.float32
    )
    gate_values = jax.nn.sigmoid(gate_logits).reshape(seq_count, blocks_dev, block_len, head_count)
    grad_rows = cotangent.reshape(seq_count, blocks_dev, block_len, head_count, head_dim)
    branch_grad = (gate_values[..., None] * grad_rows.astype(jnp.float32)).astype(jnp.bfloat16)
    row_dot = jnp.sum(branch_grad.astype(jnp.float32) * branch_out, axis=4)
    weight_grad = jnp.einsum(
        "sbqhd,sbknd->sbhqkn", branch_grad, picked_values, preferred_element_type=jnp.float32
    )
    row_dot_t = jnp.transpose(row_dot, (0, 1, 3, 2))[..., None, None]
    score_grad = (weights * (weight_grad - row_dot_t) * score_scale).astype(jnp.bfloat16)
    query_grad = jnp.einsum(
        "sbhqkn,sbknd->sbqhd", score_grad, picked_keys, preferred_element_type=jnp.float32
    )
    query_grad = query_grad.astype(jnp.bfloat16).reshape(seq_count, tok_rows, row_width)
    pick_key = jnp.einsum(
        "sbhqkn,sbqhd->sbknd", score_grad, query_rows, preferred_element_type=jnp.float32
    )
    pick_value = jnp.einsum(
        "sbhqkn,sbqhd->sbknd", weights_bf, branch_grad, preferred_element_type=jnp.float32
    )
    entry_width = block_len * 2 * head_dim
    flat_grads = jnp.concatenate([pick_key, pick_value], axis=-1).reshape(
        seq_count, blocks_dev * pick_count, entry_width
    )
    flat_ids = chosen_ids.reshape(seq_count, blocks_dev * pick_count)
    block_range = jnp.arange(blocks_dev, dtype=jnp.int32)
    holder = flat_ids // blocks_dev
    within = flat_ids % blocks_dev
    at_home = holder == own_index
    earlier = holder < own_index
    home_hits = (at_home[..., None] & (within[..., None] == block_range)).astype(jnp.float32)
    own_sum = jnp.einsum("spc,spe->cse", home_hits, flat_grads, precision=lax.Precision.HIGHEST)
    visited = (flat_ids[..., None] == jnp.arange(total_blocks, dtype=jnp.int32)) & earlier[
        ..., None
    ]
    visited = jnp.max(visited.astype(jnp.int32), axis=1).reshape(seq_count, devices, blocks_dev)
    slot_of = jnp.cumsum(visited, axis=2) - 1
    pick_slot = jnp.take_along_axis(slot_of.reshape(seq_count, total_blocks), flat_ids, axis=1)
    target = holder * MOST + pick_slot
    slot_range = jnp.arange(devices * MOST, dtype=jnp.int32)
    send_hits = ((target[..., None] == slot_range) & earlier[..., None]).astype(jnp.float32)
    outgoing = jnp.einsum("spc,spe->cse", send_hits, flat_grads, precision=lax.Precision.HIGHEST)
    outgoing = outgoing.reshape(devices, MOST, seq_count, entry_width)
    matches = (visited[..., None] == 1) & (slot_of[..., None] == jnp.arange(MOST, dtype=jnp.int32))
    present = jnp.max(matches.astype(jnp.int32), axis=2)
    where_block = jnp.sum(matches.astype(jnp.int32) * block_range[:, None], axis=2)
    labels = jnp.transpose(jnp.where(present == 1, where_block, -1), (1, 2, 0))
    incoming, arrived = (
        lax.all_to_all(outgoing, "kv", split_axis=0, concat_axis=0, tiled=True),
        lax.all_to_all(labels, "kv", split_axis=0, concat_axis=0, tiled=True),
    )
    landing = (arrived[..., None] == block_range).astype(jnp.float32)
    own_sum = own_sum + jnp.einsum(
        "nmsc,nmse->cse", landing, incoming, precision=lax.Precision.HIGHEST
    )
    own_sum = own_sum.reshape(blocks_dev, seq_count, block_len, 2 * head_dim)
    own_sum = jnp.transpose(own_sum, (1, 0, 2, 3)).reshape(seq_count, tok_rows, 2 * head_dim)
    key_grad = own_sum[..., :head_dim].astype(jnp.bfloat16)
    value_grad = own_sum[..., head_dim:].astype(jnp.bfloat16)
    quarter_values = lax.all_to_all(value_grad, "tp", split_axis=1, concat_axis=2, tiled=True)
    value_weight_grad = lax.psum_scatter(
        jnp.einsum("std,ste->de", layer_input, quarter_values, preferred_element_type=jnp.float32),
        ("kv", "tp"),
        scatter_dimension=0,
        tiled=True,
    )
    return (query_grad, key_grad, value_grad, value_weight_grad)


def solution(mesh):
    in_specs = (
        P(None, "kv", "tp"),
        P(None, "kv", "tp"),
        P(None, "kv", "tp"),
        P(None, "kv", "tp"),
        P(None, "kv", "tp"),
        P(None, ("kv", "tp"), None),
        P(None, "kv", "tp", None),
    )
    out_specs = (
        P(None, "kv", "tp"),
        P(None, "kv", "tp"),
        P(None, "kv", "tp"),
        P(("kv", "tp"), None),
    )
    return jax.shard_map(
        on_device, mesh=mesh, in_specs=in_specs, out_specs=out_specs, check_vma=False
    )
```

profile of v0, /device:TPU:0, one launch (start us, length us, event | category | flops | bytes accessed | tf_op | source)
XLA Modules:
  0.0 399.5 jit_solution(10944835787153291464)
XLA Ops:
  11.2 7.3 %all-to-all-start.1 = ((s32[8,2,2]{1,2,0:T(2,128)}), s32[8,2,2]{1,2,0:T(2,128)}, u32[]{:S(2)}, u32[]{:S(2)}) async-start(s32[8,2,2]{1,2,0:T(2,128)} %copy.93), calls=%async_computation.1 | async-start | bytes 16384 | tf_op jit(solution)/shard_map/all_to_all | solution.py:98
  20.5 35.2 %all_gather.6 = bf16[2,3072,64]{1,2,0:T(8,128)(2,1)} all-gather(bf16[2,384,64]{1,2,0:T(8,128)(2,1)} %param.8), channel_id=1, replica_groups=mesh['kv'=8,'tp'=4] {'kv'}, dimensions={1}, use_global_device_ids=true | all-gather | bytes 884736 | tf_op jit(solution)/shard_map/all_gather | solution.py:21
  55.7 1.8 copy.75
  57.6 2.8 reshape.235
  60.4 2.6 copy.81
  63.1 34.3 %all_gather.7 = bf16[2,3072,64]{1,2,0:T(8,128)(2,1)} all-gather(bf16[2,384,64]{1,2,0:T(8,128)(2,1)S(1)} %copy-done.5), channel_id=1, replica_groups=mesh['kv'=8,'tp'=4] {'kv'}, dimensions={1}, use_global_device_ids=true | all-gather | bytes 884736 | tf_op jit(solution)/shard_map/all_gather | solution.py:22
  97.4 2.5 copy.79
  99.9 3.7 gather_fusion
  103.6 5.1 %gather_fusion.1 = bf16[192,64,64]{2,1,0:T(8,128)(2,1)} fusion(bf16[2,48,64,64]{3,2,1,0:T(8,128)(2,1)} %bitcast.136, s32[192]{0:T(256)S(1)} %reshape.238), kind=kCustom, calls=%fused_computation.1 | custom fusion | bytes 3147264 | tf_op jit(solution)/shard_map/gather | solution.py:30
  108.9 2.6 reshape.227
  111.7 2.3 broadcast_compare_fusion
  114.0 12.2 %fusion.5 = (f32[2,6,4,64]{3,2,1,0:T(4,128)S(1)}, f32[2,6,16,64,64,4]{4,3,5,2,1,0:T(8,128)}) fusion(pred[2,6,64,16,64]{2,4,3,1,0:T(8,128)(4,1)S(1)} %broadcast_compare_fusion, bf16[2,6,16,64,64,1]{4,3,5,2,1,0:T(8,128)(2,1)} %bitcast.133, bf16[2,6,64,4,64,1]{4,3,2,1,0,5:T(4,128)(2,1)} %bitcast.137), kind=kOutput, calls=%fused_computation.11 | convolution fusion | flops 412087296 | bytes 15347712 | tf_op jit(solution)/shard_map/sbqhd,sbknd->sbhqkn/dot_general | solution.py:33
  126.2 11.8 %fusion.4 = f32[2,6,4,64]{3,2,1,0:T(4,128)S(1)} fusion(f32[2,6,16,64,64,4]{4,3,5,2,1,0:T(8,128)} %get-tuple-element.31, f32[2,6,4,64]{3,2,1,0:T(4,128)S(1)} %get-tuple-element.30, pred[2,6,64,16,64]{2,4,3,1,0:T(8,128)(4,1)S(1)} %broadcast_compare_fusion), kind=kLoop, calls=%fused_computation.10 | loop fusion | flops 12579840 | bytes 13393920 | tf_op jit(solution)/shard_map/reduce_sum | solution.py:45
  138.0 12.9 %fusion.12 = f32[2,6,16,64,64]{4,3,2,1,0:T(8,128)} fusion(bf16[2,6,64,4,64]{2,4,3,1,0:T(8,128)(2,1)S(1)} %multiply_convert_fusion, f32[2,6,16,64,64,4]{4,3,5,2,1,0:T(8,128)} %get-tuple-element.31, f32[2,6,4,64]{3,2,1,0:T(4,128)S(1)} %fusion.4, f32[2,6,4,64]{3,2,1,0:T(4,128)S(1)} %get-tuple-element.30, pred[2,6,64,16,64]{2,4,3,1,0:T(8,128)(4,1)S(1)} %broadcast_compare_fusion), kind=kOutput, calls=%fused_computation.24 | convolution fusion | flops 418381824 | bytes 16932864 | tf_op jit(solution)/shard_map/sbhqkn,sbqhd->sbknd/dot_general | solution.py:66
  150.9 13.5 %fusion.15 = f32[2,6,64,4]{2,3,1,0:T(4,128)S(1)} fusion(bf16[2,6,64,4,64]{2,4,3,1,0:T(8,128)(2,1)} %copy-done.4, bf16[2,6,16,64,64,1]{4,3,5,2,1,0:T(8,128)(2,1)} %bitcast.139, f32[2,6,16,64,64,4]{4,3,5,2,1,0:T(8,128)} %get-tuple-element.31, f32[2,6,4,64]{3,2,1,0:T(4,128)S(1)} %fusion.4, f32[2,6,4,64]{3,2,1,0:T(4,128)S(1)} %get-tuple-element.30, ...), kind=kOutput, calls=%fused_computation.28 | convolution fusion | flops 418968576 | bytes 15372288 | tf_op jit(solution)/shard_map/sbhqkn,sbknd->sbqhd/dot_general | solution.py:47
  164.4 17.0 %fusion.2 = bf16[2,6,4,64,16,64]{3,5,2,4,1,0:T(8,128)(2,1)} fusion(f32[2,6,4,64]{3,2,1,0:T(4,128)S(1)} %bitcast.146, bf16[2,6,16,64,64,1]{4,3,5,2,1,0:T(8,128)(2,1)} %bitcast.140, bf16[2,6,64,4,64]{2,4,3,1,0:T(8,128)(2,1)} %copy-done.4, f32[2,6,4,64]{3,2,1,0:T(4,128)S(1)} %fusion.4, f32[2,6,4,64]{3,2,1,0:T(4,128)S(1)} %get-tuple-element.30, ...), kind=kOutput, calls=%fused_computation.6 | convolution fusion | flops 427819008 | bytes 21663744 | tf_op jit(solution)/shard_map/sbqhd,sbknd->sbhqkn/dot_general | solution.py:54
  181.4 7.3 %convolution_bitcast_fusion.3 = f32[2,6,16,64,64]{4,3,2,1,0:T(8,128)S(1)} fusion(bf16[2,6,4,64,16,64]{3,5,2,4,1,0:T(8,128)(2,1)} %fusion.2, bf16[2,6,64,4,64,1]{4,3,2,1,0,5:T(4,128)(2,1)} %bitcast.138), kind=kOutput, calls=%fused_computation.25 | convolution fusion | flops 402653184 | bytes 9830400 | tf_op jit(solution)/shard_map/sbhqkn,sbqhd->sbknd/dot_general | solution.py:63
  188.8 4.3 %pad_maximum_fusion = f32[2,6,16,64,128]{4,3,2,1,0:T(8,128)} fusion(f32[2,6,16,64,64]{4,3,2,1,0:T(8,128)S(1)} %copy-done.3, f32[2,6,16,64,64]{4,3,2,1,0:T(8,128)S(1)} %convolution_bitcast_fusion.3), kind=kLoop, calls=%fused_computation.17 | loop fusion | flops 1572864 | bytes 12582912 | tf_op jit(solution)/shard_map/concatenate | solution.py:70
  193.1 7.2 %reshape.230 = f32[2,96,8192]{2,1,0:T(8,128)} reshape(f32[2,6,16,64,128]{4,3,2,1,0:T(8,128)} %pad_maximum_fusion) | data formatting | bytes 12582912 | tf_op jit(solution)/shard_map/reshape | solution.py:70
  200.4 2.0 gather_fusion.2
  202.5 5.9 %convolution_bitcast_fusion = f32[16,2,8192]{2,0,1:T(8,128)} fusion(f32[2,96,8192]{2,1,0:T(8,128)} %reshape.230, s32[2,96]{1,0:T(2,128)S(1)} %get-tuple-element.29, pred[2,96]{1,0:T(4,128)(4,1)S(1)} %copy-done.12), kind=kOutput, calls=%fused_computation.12 | convolution fusion | flops 301996032 | bytes 7340992 | tf_op jit(solution)/shard_map/spc,spe->cse/dot_general | solution.py:90
  208.4 1.8 reshape.232
  210.3 1.0 copy.90
  211.3 5.5 %all-to-all-start = ((f32[8,2,2,8192]{3,1,2,0:T(2,128)}), f32[8,2,2,8192]{3,1,2,0:T(2,128)S(1)}, u32[]{:S(2)}, u32[]{:S(2)}) async-start(f32[8,2,2,8192]{3,1,2,0:T(2,128)} %copy.90), calls=%async_computation | async-start | bytes 2097152 | tf_op jit(solution)/shard_map/all_to_all | solution.py:97
  217.8 15.4 %all-to-all-done = f32[8,2,2,8192]{3,1,2,0:T(2,128)S(1)} async-done(((f32[8,2,2,8192]{3,1,2,0:T(2,128)}), f32[8,2,2,8192]{3,1,2,0:T(2,128)S(1)}, u32[]{:S(2)}, u32[]{:S(2)}) %all-to-all-start) | async-done | bytes 1048608 | tf_op jit(solution)/shard_map/all_to_all | solution.py:97
  234.2 4.9 %fusion.7 = bf16[6,2,8192]{2,0,1:T(8,128)(2,1)S(1)} fusion(f32[2,8192,6]{1,2,0:T(8,128)S(1)} %convolution_bitcast_fusion.1, f32[2,96,8192]{2,1,0:T(8,128)} %reshape.230, s32[2,96]{1,0:T(2,128)S(1)} %get-tuple-element.28, pred[2,96]{1,0:T(4,128)(4,1)S(1)} %copy-done.14), kind=kOutput, calls=%fused_computation.16 | convolution fusion | flops 113445120 | bytes 6882240 | tf_op jit(solution)/shard_map/spc,spe->cse/dot_general | solution.py:80
  240.0 6.9 %all_to_all.28 = bf16[4,2,6144]{2,1,0:T(2,128)(2,1)S(1)} all-to-all(bf16[4,2,6144]{2,1,0:T(2,128)(2,1)S(1)} %reshape.274), channel_id=1, replica_groups=mesh['kv'=8,'tp'=4] {'tp'}, dimensions={0} | all-to-all | bytes 196608 | tf_op jit(solution)/shard_map/all_to_all | solution.py:108
  247.2 2.7 convolution_bitcast_fusion.2
  249.9 7.9 %fusion.18 = bf16[2,6,64,4,64]{2,4,3,1,0:T(8,128)(2,1)S(1)} fusion(bf16[2,6,16,64,64,1]{4,3,5,2,1,0:T(8,128)(2,1)} %bitcast.134, bf16[2,6,4,64,16,64]{3,5,2,4,1,0:T(8,128)(2,1)} %fusion.2), kind=kOutput, calls=%fused_computation.30 | convolution fusion | flops 402849792 | bytes 8257536 | tf_op jit(solution)/shard_map/sbhqkn,sbknd->sbqhd/dot_general | solution.py:59
  258.4 1.2 reshape.229
  261.2 129.6 %reduce-scatter.2.cloned.1.call-done = f32[128,256]{0,1:T(8,128)} async-done(((f32[4096,256]{0,1:T(8,128)}), f32[128,256]{0,1:T(8,128)}) %reduce-scatter.2.cloned.1.call-update) | async-done | bytes 131088 | tf_op jit(solution)/shard_map/reduce_scatter | solution.py:109
  390.7 1.7 copy.103
  (75 shorter events, 12.1 us)
Async XLA Ops:
  7.2 240.0 %copy-start = (bf16[2,96,4096]{2,1,0:T(8,128)(2,1)S(1)}, bf16[2,96,4096]{2,1,0:T(8,128)(2,1)}, u32[]{:S(2)}) copy-start(bf16[2,96,4096]{2,1,0:T(8,128)(2,1)} %param.12) | copy-start | bytes 4718596
  7.2 55.8 %copy-start.8 = (f32[2,384,4]{1,2,0:T(4,128)S(1)}, f32[2,384,4]{1,2,0:T(4,128)}, u32[]{:S(2)}) copy-start(f32[2,384,4]{1,2,0:T(4,128)} %param.11) | copy-start | bytes 36868
  7.2 55.9 %copy-start.5 = (bf16[2,384,64]{1,2,0:T(8,128)(2,1)S(1)}, bf16[2,384,64]{1,2,0:T(8,128)(2,1)}, u32[]{:S(2)}) copy-start(bf16[2,384,64]{1,2,0:T(8,128)(2,1)} %param.9) | copy-start | bytes 294916
  8.1 0.6 copy-start.6
  8.7 0.6 copy-start.9
  9.3 0.5 copy-start.11
  11.2 200.1 %all-to-all-start.1 = ((s32[8,2,2]{1,2,0:T(2,128)}), s32[8,2,2]{1,2,0:T(2,128)}, u32[]{:S(2)}, u32[]{:S(2)}) async-start(s32[8,2,2]{1,2,0:T(2,128)} %copy.93), calls=%async_computation.1 | async-start | bytes 16384 | tf_op jit(solution)/shard_map/all_to_all | solution.py:98
  103.6 7.9 %copy-start.2 = (f32[2,6,64,4,64]{2,4,3,1,0:T(8,128)S(1)}, f32[2,6,64,4,64]{2,4,3,1,0:T(8,128)}, u32[]{:S(2)}) copy-start(f32[2,6,64,4,64]{2,4,3,1,0:T(8,128)} %copy.81) | copy-start | bytes 2359300
  111.7 26.3 %copy-start.4 = (bf16[2,6,64,4,64]{2,4,3,1,0:T(8,128)(2,1)}, bf16[2,6,64,4,64]{2,4,3,1,0:T(8,128)(2,1)S(1)}, u32[]{:S(2)}) copy-start(bf16[2,6,64,4,64]{2,4,3,1,0:T(8,128)(2,1)S(1)} %multiply_convert_fusion) | copy-start | bytes 1179652
  181.4 7.4 %copy-start.3 = (f32[2,6,16,64,64]{4,3,2,1,0:T(8,128)S(1)}, f32[2,6,16,64,64]{4,3,2,1,0:T(8,128)}, u32[]{:S(2)}) copy-start(f32[2,6,16,64,64]{4,3,2,1,0:T(8,128)} %fusion.12) | copy-start | bytes 9437188
  193.1 7.2 %copy-start.13 = (s32[2,96,1]{1,0,2:T(2,128)S(1)}, s32[2,96,1]{1,0,2:T(2,128)}, u32[]{:S(2)}) copy-start(s32[2,96,1]{1,0,2:T(2,128)} %reshape_squeeze.6) | copy-start | bytes 2308
  193.1 7.3 %copy-start.1 = (s32[2,48]{1,0:T(2,128)S(1)}, s32[2,48]{1,0:T(2,128)}, u32[]{:S(2)}) copy-start(s32[2,48]{1,0:T(2,128)} %sub.34) | copy-start | bytes 1156
  193.1 9.4 %copy-start.7 = (s32[2,96]{1,0:T(2,128)S(1)}, s32[2,96]{1,0:T(2,128)}, u32[]{:S(2)}) copy-start(s32[2,96]{1,0:T(2,128)} %copy-done.6) | copy-start | bytes 2308
  193.1 9.4 %copy-start.10 = (s32[2,96]{1,0:T(2,128)S(1)}, s32[2,96]{1,0:T(2,128)}, u32[]{:S(2)}) copy-start(s32[2,96]{1,0:T(2,128)} %copy-done.9) | copy-start | bytes 2308
  193.1 9.4 %copy-start.12 = (pred[2,96]{1,0:T(4,128)(4,1)S(1)}, pred[2,96]{1,0:T(4,128)(4,1)}, u32[]{:S(2)}) copy-start(pred[2,96]{1,0:T(4,128)(4,1)} %copy-done.11) | copy-start | bytes 580
  202.5 31.7 %copy-start.14 = (pred[2,96]{1,0:T(4,128)(4,1)S(1)}, pred[2,96]{1,0:T(4,128)(4,1)}, u32[]{:S(2)}) copy-start(pred[2,96]{1,0:T(4,128)(4,1)} %get-tuple-element.22) | copy-start | bytes 580
  211.3 21.9 %all-to-all-start = ((f32[8,2,2,8192]{3,1,2,0:T(2,128)}), f32[8,2,2,8192]{3,1,2,0:T(2,128)S(1)}, u32[]{:S(2)}, u32[]{:S(2)}) async-start(f32[8,2,2,8192]{3,1,2,0:T(2,128)} %copy.90), calls=%async_computation | async-start | bytes 2097152 | tf_op jit(solution)/shard_map/all_to_all | solution.py:97
  216.8 173.9 %reduce-scatter.2.cloned.1.call-start = ((), (), s32[]{:S(2)}) async-start(), calls=%async_computation.4 | async-start | bytes 4325376 | tf_op jit(solution)/shard_map/reduce_scatter | solution.py:109
Sparse Core Ops, SparseCore 0:
  250.0 140.6 reduce-scatter.1
where the time goes:
time: 402 us; the launch traced here: 399 us
  waiting for transfers between devices  145 us (36%)
  matrix products  85.3 us (21%)
  blocking collectives  76.3 us (19%)
  local copies, waits for them, and re-layouts  43.8 us (11%)
  other arithmetic  21.5 us (5%)
  between operations  14.5 us (4%)
  starting transfers between devices  13.1 us (3%)
    reduce_scatter x1, waiting for transfers between devices, on_device(): lax.psum_scatter(jnp.einsum('std,ste->de', layer_input, quarter_values, p...  130 us
    all_gather x1, blocking collectives, on_device(): lax.all_gather(key_states, 'kv', axis=1, tiled=True)  35.2 us
    all_gather x1, blocking collectives, on_device(): lax.all_gather(value_states, 'kv', axis=1, tiled=True)  34.3 us
    dot_general x1, matrix products, on_device(): jnp.einsum('sbqhd,sbknd->sbhqkn', branch_grad, picked_values, preferred_e...  17 us
    all_to_all x1, waiting for transfers between devices, on_device(): lax.all_to_all(outgoing, 'kv', split_axis=0, concat_axis=0, tiled=True)  15.4 us
    dot_general x1, matrix products, on_device(): jnp.einsum('sbhqkn,sbknd->sbqhd', weights_bf, picked_values, preferred_el...  13.5 us
    dot_general x1, matrix products, on_device(): jnp.einsum('sbhqkn,sbqhd->sbknd', weights_bf, branch_grad, preferred_elem...  12.9 us
    dot_general x1, matrix products, on_device(): jnp.einsum('sbqhd,sbknd->sbhqkn', query_rows, picked_keys, preferred_elem...  12.2 us
  transfers between devices with their start and end apart: 3, of which 2 were waited for; matrix products, arithmetic and copies ran while one was open for 34% of the time, Pallas kernels for 0%

commit v1 on v0

v1 whole, which is shorter than its diff:
```python
import functools
import math

import jax
import jax.numpy as jnp
from jax import lax
from jax.experimental import pallas as pl
from jax.experimental.pallas import tpu as pltpu
from jax.sharding import PartitionSpec as P

BLK = 64
MOST = 2
LABEL_ROWS = 16
LOG2E = math.log2(math.e)
BF = jnp.bfloat16
F32 = jnp.float32
VMEM = pltpu.VMEM
SMEM = pltpu.SMEM
BIG_VMEM = pltpu.CompilerParams(vmem_limit_bytes=56 * 1024 * 1024)


def vspec():
    return pl.BlockSpec(memory_space=VMEM)


def sspec():
    return pl.BlockSpec(memory_space=SMEM)


def prep_kernel(heads, hd, scale, q_ref, g_ref, gate_ref, r_ref):
    width = 2 * hd
    rows = heads * BLK
    low = lax.broadcasted_iota(jnp.int32, (BLK, width), 1) < hd

    def step(i, carry):
        at = pl.ds(pl.multiple_of(i * BLK, BLK), BLK)
        gates = jax.nn.sigmoid(gate_ref[at, :])
        for pair in range(heads // 2):
            q = q_ref[at, pair * width : (pair + 1) * width].astype(F32) * scale
            g = g_ref[at, pair * width : (pair + 1) * width].astype(F32)
            gv = jnp.where(low, gates[:, 2 * pair : 2 * pair + 1], gates[:, 2 * pair + 1 : 2 * pair + 2])
            g = g * gv
            qr = pltpu.roll(q, hd, 1)
            gr = pltpu.roll(g, hd, 1)
            zero = jnp.zeros_like(q)
            base = 2 * pair * BLK
            r_ref[i, base : base + BLK, :] = jnp.where(low, q, zero).astype(BF)
            r_ref[i, base + BLK : base + 2 * BLK, :] = jnp.where(low, qr, zero).astype(BF)
            r_ref[i, rows + base : rows + base + BLK, :] = jnp.where(low, zero, gr).astype(BF)
            r_ref[i, rows + base + BLK : rows + base + 2 * BLK, :] = jnp.where(low, zero, g).astype(BF)
        return carry

    lax.fori_loop(0, q_ref.shape[0] // BLK, step, 0)


def pack_kernel(seqs, bpd, shifts, *refs):
    labels = refs[:shifts]
    pair_ref = refs[shifts]
    outs = refs[shifts + 1 :]
    for d in range(shifts):
        for s in range(seqs):
            for yh in range(2):
                for m in range(MOST):
                    slot = (s * 2 + yh) * MOST + m
                    lab = labels[d][d * seqs * 2 * MOST + slot]
                    src = pl.multiple_of(((yh * seqs + s) * bpd + lab) * BLK, BLK)
                    outs[d][slot * BLK : (slot + 1) * BLK, :] = pair_ref[pl.ds(src, BLK), :]


def attend_kernel(
    nblk, bpd, heads, hd, picks, shifts, zshifts, scale, kv_loc, acc_loc, labs, r_ref, pair_ref, *refs
):
    zmsgs = refs[:zshifts]
    dq_ref, own_ref = refs[zshifts : zshifts + 2]
    outs = refs[zshifts + 2 : zshifts + 2 + shifts]
    kv_all, kv_pick, s_buf, p_buf, x_buf, acc, dq_buf = refs[zshifts + 2 + shifts :]
    rows = heads * BLK
    width = 2 * hd
    seqs = nblk // bpd
    slots = seqs * MOST
    dummy = nblk + shifts * slots
    chunk = 4 * BLK
    keys = picks * BLK

    pair_rows = pair_ref.shape[0]
    kv_all[0:pair_rows, :] = pair_ref[...]
    for d in range(zshifts):
        n = zmsgs[d].shape[0]
        kv_all[pair_rows + d * n : pair_rows + (d + 1) * n, :] = zmsgs[d][...]
    acc[...] = jnp.zeros_like(acc)
    kpos = lax.broadcasted_iota(jnp.int32, (BLK, rows), 0)
    qpos = lax.broadcasted_iota(jnp.int32, (BLK, rows), 1) % BLK
    diag = kpos <= qpos

    def fold(x, op):
        out = x[0:8, :]
        for i in range(1, x.shape[0] // 8):
            out = op(out, x[i * 8 : (i + 1) * 8, :])
        return out

    def step(i, carry):
        base = i * picks
        for j in range(picks):
            src = pl.multiple_of(kv_loc[base + j] * BLK, BLK)
            kv_pick[j * BLK : (j + 1) * BLK, :] = kv_all[pl.ds(src, BLK), :]
        r = r_ref[i]
        top = jnp.full((8, rows), -jnp.inf, F32)
        for c in range(keys // chunk):
            both = lax.dot_general(
                kv_pick[c * chunk : (c + 1) * chunk, :], r, (((1,), (1,)), ((), ())), preferred_element_type=F32
            )
            p_buf[c * chunk : (c + 1) * chunk, :] = both[:, rows:]
            for j in range(4):
                pick = c * 4 + j
                s = both[j * BLK : (j + 1) * BLK, :rows] * LOG2E
                if pick == 0:
                    s = jnp.where(diag, s, -jnp.inf)
                else:
                    bias = jnp.where(acc_loc[base + pick] == dummy, -jnp.inf, 0.0).astype(F32)
                    s = s + bias
                s_buf[pick * BLK : (pick + 1) * BLK, :] = s
                top = jnp.maximum(top, fold(s, jnp.maximum))
        top = jnp.max(top, axis=0, keepdims=True)
        total = jnp.zeros((8, rows), F32)
        for j in range(picks):
            e = jnp.exp2(s_buf[j * BLK : (j + 1) * BLK, :] - top)
            total = total + fold(e, jnp.add)
        shift = top + jnp.log2(jnp.sum(total, axis=0, keepdims=True))
        dot = jnp.zeros((8, rows), F32)
        for j in range(picks):
            at = slice(j * BLK, (j + 1) * BLK)
            w = jnp.exp2(s_buf[at, :] - shift)
            wb = w.astype(BF)
            s_buf[at, :] = w
            x_buf[at, rows:] = wb
            dot = dot + fold(wb.astype(F32) * p_buf[at, :], jnp.add)
        dot = jnp.sum(dot, axis=0, keepdims=True)
        dqt = jnp.zeros((width, rows), F32)
        for c in range(keys // chunk):
            for j in range(4):
                at = slice((c * 4 + j) * BLK, (c * 4 + j + 1) * BLK)
                x_buf[at, :rows] = (s_buf[at, :] * (p_buf[at, :] - dot)).astype(BF)
            at = slice(c * chunk, (c + 1) * chunk)
            x = x_buf[at, :]
            grads = lax.dot_general(x, r, (((1,), (0,)), ((), ())), preferred_element_type=F32)
            for j in range(4):
                dst = pl.multiple_of(acc_loc[base + c * 4 + j] * BLK, BLK)
                acc[pl.ds(dst, BLK), :] += grads[j * BLK : (j + 1) * BLK, :]
            dqt = dqt + lax.dot_general(
                kv_pick[at, :], x[:, :rows], (((0,), (0,)), ((), ())), preferred_element_type=F32
            )
        dq_buf[...] = dqt[:hd, :] * scale
        row_at = pl.ds(pl.multiple_of(i * BLK, BLK), BLK)
        for pair in range(heads // 2):
            two = jnp.concatenate(
                [dq_buf[:, 2 * pair * BLK : (2 * pair + 1) * BLK], dq_buf[:, (2 * pair + 1) * BLK : (2 * pair + 2) * BLK]],
                axis=0,
            )
            dq_ref[row_at, pair * width : (pair + 1) * width] = two.T.astype(BF)
        return carry

    lax.fori_loop(0, nblk, step, 0)
    own_ref[...] = acc[0 : nblk * BLK, :]
    for d in range(shifts):
        lo = (nblk + d * slots) * BLK
        outs[d][0 : slots * BLK, :] = acc[lo : lo + slots * BLK, :].astype(BF)
        lane = lax.broadcasted_iota(jnp.int32, (LABEL_ROWS, width), 0)
        mark = jnp.zeros((LABEL_ROWS, width), F32)
        for k in range(slots):
            mark = jnp.where(lane == k, labs[d * slots + k].astype(F32), mark)
        outs[d][slots * BLK : slots * BLK + LABEL_ROWS, :] = mark.astype(BF)


def combine_kernel(seqs, bpd, hd, shifts, parts, quarter, own_ref, *refs):
    msgs = refs[:shifts]
    pieces = refs[shifts : shifts + parts]
    kg_ref, vg_ref, out_ref, total, vbuf = refs[shifts + parts :]
    slots = seqs * MOST
    total[...] = own_ref[...]
    width = 2 * hd
    for d in range(shifts):
        marks = msgs[d][slots * BLK : slots * BLK + LABEL_ROWS, :].astype(F32)
        for s in range(seqs):
            for m in range(MOST):
                k = s * MOST + m
                val = msgs[d][k * BLK : (k + 1) * BLK, :].astype(F32)
                mark = marks[k : k + 1, :]
                for b in range(bpd):
                    at = slice((s * bpd + b) * BLK, (s * bpd + b + 1) * BLK)
                    total[at, :] = total[at, :] + jnp.where(mark == float(b), val, 0.0)
    tok = bpd * BLK
    kg_ref[...] = total[:, :hd].astype(BF)
    vg = total[:, hd:].astype(BF)
    vg_ref[...] = vg
    vbuf[...] = vg
    span = tok // parts
    acc = None
    for j in range(parts):
        who = jnp.bitwise_xor(quarter[0], j)
        for s in range(seqs):
            lo = pl.multiple_of(s * tok + who * span, 16)
            v = vbuf[pl.ds(lo, span), :]
            one = lax.dot_general(
                v, pieces[j][s], (((0,), (0,)), ((), ())), preferred_element_type=F32
            )
            acc = one if acc is None else acc + one
    lanes = out_ref.shape[2]
    for i in range(out_ref.shape[0]):
        out_ref[i] = acc[:, i * lanes : (i + 1) * lanes].astype(BF)


def final_kernel(n, parts, in_ref, out_ref):
    for t in range(parts):
        acc = in_ref[t].astype(F32)
        for k in range(1, n):
            acc = acc + in_ref[k * parts + t].astype(F32)
        if t % 2 == 0:
            held = acc
        else:
            both = jnp.concatenate([held, acc], axis=0)
            w = both.shape[0]
            out_ref[:, (t // 2) * w : (t // 2 + 1) * w] = both.T


def on_device(queries, key_states, value_states, cotangent, gate_logits, layer_input, chosen):
    seqs, tok, row_width = queries.shape
    hd = key_states.shape[2]
    heads = row_width // hd
    bpd = tok // BLK
    picks = chosen.shape[3]
    n = lax.axis_size("kv")
    parts = lax.axis_size("tp")
    own = lax.axis_index("kv").astype(jnp.int32)
    t_own = lax.axis_index("tp").astype(jnp.int32)
    scale = hd ** (-0.5)
    assert math.log2(scale).is_integer() and n % 2 == 0
    nblk = seqs * bpd
    slots = seqs * MOST
    shifts = n - 1
    zshifts = n // 2 - 1
    width = 2 * hd

    perm = lambda x, axis, pairs: lax.ppermute(x, axis, pairs)
    tp_xor = lambda j: [(i, i ^ j) for i in range(parts)]
    piece2 = perm(layer_input, "tp", tp_xor(2))
    piece1 = perm(layer_input, "tp", tp_xor(1))
    piece3 = perm(piece2, "tp", tp_xor(1))
    pieces = [layer_input, piece1, piece2, piece3]

    ids = chosen[:, :, 0, :]
    flat = ids.reshape(seqs, bpd * picks)
    holder = flat // bpd
    within = flat % bpd

    dz = jnp.arange(1, zshifts + 1, dtype=jnp.int32)[:, None, None, None]
    yh = jnp.arange(2, dtype=jnp.int32)[None, None, :, None]
    target = 2 * (own // 2 - dz) + yh
    hit = holder[None, :, None, :] == target
    low = jnp.min(jnp.where(hit, within[None, :, None, :], bpd - 1), axis=-1)
    high = jnp.max(jnp.where(hit, within[None, :, None, :], 0), axis=-1)
    ask = jnp.stack([low, high], axis=-1).reshape(zshifts * seqs * 2 * MOST)
    asked = [
        perm(ask, "kv", [(k, k - 2 * d) for k in range(2 * d, n)]) for d in range(1, zshifts + 1)
    ]

    kv = jnp.concatenate([key_states, value_states], axis=-1).reshape(nblk * BLK, width)
    partner = perm(kv, "kv", [(k, k ^ 1) for k in range(n)])
    even = own % 2 == 0
    pair = jnp.where(even, jnp.concatenate([kv, partner]), jnp.concatenate([partner, kv]))

    zrows = slots * 2 * BLK
    packed = pl.pallas_call(
        functools.partial(pack_kernel, seqs, bpd, zshifts),
        out_shape=[jax.ShapeDtypeStruct((zrows, width), BF)] * zshifts,
        in_specs=[sspec()] * zshifts + [vspec()],
        out_specs=[vspec()] * zshifts,
        name="pack",
    )(*asked, pair)
    zmsgs = [
        perm(packed[d - 1], "kv", [(k, k + 2 * d) for k in range(n - 2 * d)]) for d in range(1, zshifts + 1)
    ]

    r = pl.pallas_call(
        functools.partial(prep_kernel, heads, hd, scale),
        out_shape=jax.ShapeDtypeStruct((nblk, 2 * heads * BLK, width), BF),
        in_specs=[vspec()] * 3,
        out_specs=vspec(),
        name="prep",
    )(
        queries.reshape(seqs * tok, row_width),
        cotangent.reshape(seqs * tok, row_width),
        gate_logits.reshape(seqs * tok, heads),
    )

    block = own * bpd + jnp.arange(bpd, dtype=jnp.int32)[None, :, None]
    first = ids[:, :, :1]
    at0 = lax.broadcasted_iota(jnp.int32, ids.shape, 2) == 0
    order = jnp.where(at0, block, jnp.where(ids == block, first, ids))
    h_of = order // bpd
    w_of = order % bpd
    low_of = jnp.min(
        jnp.where(h_of[..., None] == holder[:, None, None, :], within[:, None, None, :], bpd), axis=-1
    )
    slot = (w_of != low_of).astype(jnp.int32)
    seq = jnp.arange(seqs, dtype=jnp.int32)[:, None, None]
    in_pair = (h_of // 2) == (own // 2)
    z_at = 2 * nblk + ((own // 2 - h_of // 2 - 1) * seqs + seq) * 2 * MOST + (h_of % 2) * MOST + slot
    pair_at = ((h_of % 2) * seqs + seq) * bpd + w_of
    future = order > block
    kv_loc = jnp.where(future, 0, jnp.where(in_pair, pair_at, z_at)).reshape(-1)
    dummy = nblk + shifts * slots
    remote_at = nblk + ((own - h_of - 1) * seqs + seq) * MOST + slot
    acc_loc = jnp.where(future, dummy, jnp.where(h_of == own, seq * bpd + w_of, remote_at)).reshape(-1)
    back = own - jnp.arange(1, n, dtype=jnp.int32)[:, None, None]
    hit = holder[None] == back
    low = jnp.min(jnp.where(hit, within[None], bpd - 1), axis=-1)
    high = jnp.max(jnp.where(hit, within[None], 0), axis=-1)
    labs = jnp.stack([low, high], axis=-1).reshape(shifts * slots)

    keys = picks * BLK
    rows = heads * BLK
    mrows = slots * BLK + LABEL_ROWS
    attended = pl.pallas_call(
        functools.partial(attend_kernel, nblk, bpd, heads, hd, picks, shifts, zshifts, scale),
        out_shape=[
            jax.ShapeDtypeStruct((seqs * tok, row_width), BF),
            jax.ShapeDtypeStruct((nblk * BLK, width), F32),
        ]
        + [jax.ShapeDtypeStruct((mrows, width), BF)] * shifts,
        in_specs=[sspec()] * 3 + [vspec()] * (2 + zshifts),
        out_specs=[vspec()] * (2 + shifts),
        scratch_shapes=[
            VMEM((2 * nblk * BLK + zshifts * zrows, width), BF),
            VMEM((keys, width), BF),
            VMEM((keys, rows), F32),
            VMEM((keys, rows), F32),
            VMEM((keys, 2 * rows), BF),
            VMEM(((dummy + 1) * BLK, width), F32),
            VMEM((hd, rows), F32),
        ],
        compiler_params=BIG_VMEM,
        name="attend",
    )(kv_loc, acc_loc, labs, r, pair, *zmsgs)
    query_grad = attended[0].reshape(seqs, tok, row_width)
    own_sum = attended[1]
    arrived = [
        perm(attended[1 + d], "kv", [(k, k - d) for k in range(d, n)]) for d in range(1, n)
    ]

    ranks = n * parts
    depth = layer_input.shape[2]
    share = depth // ranks
    kg, vg, partial = pl.pallas_call(
        functools.partial(combine_kernel, seqs, bpd, hd, shifts, parts),
        out_shape=[
            jax.ShapeDtypeStruct((seqs * tok, hd), BF),
            jax.ShapeDtypeStruct((seqs * tok, hd), BF),
            jax.ShapeDtypeStruct((ranks * share // 128, hd, 128), BF),
        ],
        in_specs=[sspec()] + [vspec()] * (1 + shifts + parts),
        out_specs=[vspec()] * 3,
        scratch_shapes=[VMEM((nblk * BLK, width), F32), VMEM((seqs * tok, hd), BF)],
        compiler_params=BIG_VMEM,
        name="combine",
    )(t_own.reshape(1), own_sum, *arrived, *pieces)
    key_grad = kg.reshape(seqs, tok, hd)
    value_grad = vg.reshape(seqs, tok, hd)
    if share != 128:
        partial = partial.transpose(1, 0, 2).reshape(hd, ranks, share).transpose(1, 0, 2)
    swapped = lax.all_to_all(partial, ("kv", "tp"), split_axis=0, concat_axis=0, tiled=True)
    value_weight_grad = pl.pallas_call(
        functools.partial(final_kernel, n, parts),
        out_shape=jax.ShapeDtypeStruct((share, parts * hd), F32),
        in_specs=[vspec()],
        out_specs=vspec(),
        name="final",
    )(swapped)
    return query_grad, key_grad, value_grad, value_weight_grad


def solution(mesh):
    in_specs = (
        P(None, "kv", "tp"),
        P(None, "kv", "tp"),
        P(None, "kv", "tp"),
        P(None, "kv", "tp"),
        P(None, "kv", "tp"),
        P(None, ("kv", "tp"), None),
        P(None, "kv", "tp", None),
    )
    out_specs = (
        P(None, "kv", "tp"),
        P(None, "kv", "tp"),
        P(None, "kv", "tp"),
        P(("kv", "tp"), None),
    )
    return jax.shard_map(
        on_device, mesh=mesh, in_specs=in_specs, out_specs=out_specs, check_vma=False
    )
```

time: 402 us -> 159 us (0.40)
  matrix products: 85.3 us -> 0 us
  waiting for transfers between devices: 145 us -> 64 us
  blocking collectives: 76.3 us -> 0 us
  Pallas kernels: 0 us -> 35.9 us
  local copies, waits for them, and re-layouts: 43.8 us -> 18.8 us
  starting transfers between devices: 13.1 us -> 28.1 us
  between operations: 14.5 us -> 0.94 us
  other arithmetic: 21.5 us -> 9.9 us
    reduce_scatter x1 -> x0, waiting for transfers between devices: 130 us -> none  [on_device(): lax.psum_scatter(jnp.einsum('std,ste->de', layer_input, quarter_values, p...]
    dot_general x10 -> x0, matrix products: 85.3 us -> none  [the longest x1 17 us: on_device(): jnp.einsum('sbqhd,sbknd->sbhqkn', branch_grad, picked_values, preferred_e...]
    all_gather x2 -> x0, blocking collectives: 69.5 us -> none  [the longest x1 35.2 us: on_device(): lax.all_gather(key_states, 'kv', axis=1, tiled=True)]
    ppermute x0 -> x17, waiting for transfers between devices: none -> 51.7 us  [on_device(): perm = lambda x, axis, pairs: lax.ppermute(x, axis, pairs)]
    pallas_call x0 -> x5, Pallas kernels: none -> 35.9 us  [the longest x1 21.9 us: on_device(): pl.pallas_call(functools.partial(attend_kernel, nblk, bpd, heads, hd, pic...]
    ppermute x0 -> x17, starting transfers between devices: none -> 25.5 us  [on_device(): perm = lambda x, axis, pairs: lax.ppermute(x, axis, pairs)]
    reshape x6 -> x2, local copies, waits for them, and re-layouts: 14 us -> 1.25 us  [the longest x1 0.63 us: on_device(): labs = jnp.stack([low, high], axis=-1).reshape(shifts * slots)]
    reduce_sum x1 -> x0, other arithmetic: 11.8 us -> none  [on_device(): weights = exp_terms / jnp.sum(exp_terms, axis=(4, 5), keepdims=True)]
  transfers between devices with their start and end apart: 3 -> 18, of which waited for: 2 -> 11; matrix products, arithmetic and copies ran while one was open for 34% -> 16% of each run, Pallas kernels for 0% -> 18%
where the time goes in v1:
time: 159 us; the launch traced here: 158 us
  waiting for transfers between devices  64 us (40%)
  Pallas kernels  35.9 us (23%)
  starting transfers between devices  28.1 us (18%)
  local copies, waits for them, and re-layouts  18.8 us (12%)
  other arithmetic  9.9 us (6%)
    ppermute x17, waiting for transfers between devices, on_device(): perm = lambda x, axis, pairs: lax.ppermute(x, axis, pairs)  51.7 us
    ppermute x17, starting transfers between devices, on_device(): perm = lambda x, axis, pairs: lax.ppermute(x, axis, pairs)  25.5 us
    pallas_call x1, Pallas kernels, on_device(): pl.pallas_call(functools.partial(attend_kernel, nblk, bpd, heads, hd, pic...  21.9 us
    all_to_all x1, waiting for transfers between devices, on_device(): lax.all_to_all(partial, ('kv', 'tp'), split_axis=0, concat_axis=0, tiled=...  12.2 us
    unnamed x44, local copies, waits for them, and re-layouts  8.86 us
    pallas_call x1, Pallas kernels, on_device(): pl.pallas_call(functools.partial(combine_kernel, seqs, bpd, hd, shifts, p...  5.78 us
    pallas_call x1, Pallas kernels, on_device(): pl.pallas_call(functools.partial(prep_kernel, heads, hd, scale), out_shap...  4.6 us
  transfers between devices with their start and end apart: 18, of which 11 were waited for; matrix products, arithmetic and copies ran while one was open for 16% of the time, Pallas kernels for 18%

profile of v1, /device:TPU:0, one launch (start us, length us, event | category | flops | bytes accessed | tf_op | source)
XLA Modules:
  0.0 157.6 jit_solution(8787959333739067148)
XLA Ops:
  0.6 3.0 %collective-permute-start.15 = (bf16[2,96,4096]{2,1,0:T(8,128)(2,1)}, bf16[2,96,4096]{2,1,0:T(8,128)(2,1)S(1)}, u32[]{:S(2)}, u32[]{:S(2)}) collective-permute-start(bf16[2,96,4096]{2,1,0:T(8,128)(2,1)} %refs_7_.1), channel_id=1, source_target_pairs={{0,2},{1,3},{2,0},{3,1},{4,6},{5,7},{6,4},{7,5},{8,10},{9,11},{10,... | collective-permute-start | bytes 4718600 | tf_op jit(solution)/shard_map/ppermute | solution.py:243
  4.5 1.4 divide_reduce_fusion
  8.7 1.3 collective-permute-start.2
  11.2 1.6 %collective-permute-start = (bf16[768,128]{1,0:T(8,128)(2,1)S(1)}, bf16[768,128]{1,0:T(8,128)(2,1)S(1)}, u32[]{:S(2)}, u32[]{:S(2)}) collective-permute-start(bf16[768,128]{1,0:T(8,128)(2,1)S(1)} %bitcast.20), channel_id=1, source_target_pairs={{0,4},{4,0},{8,12},{12,8},{16,20},{20,16},{24,28},{28,24},{1,5},{5... | collective-permute-start | bytes 589832 | tf_op jit(solution)/shard_map/ppermute | solution.py:243
  13.7 24.5 %collective-permute-done.15.refs_9_ = bf16[2,96,4096]{2,1,0:T(8,128)(2,1)S(1)} collective-permute-done((bf16[2,96,4096]{2,1,0:T(8,128)(2,1)}, bf16[2,96,4096]{2,1,0:T(8,128)(2,1)S(1)}, u32[]{:S(2)}, u32[]{:S(2)}) %collective-permute-start.15) | collective-permute-done | bytes 1572896 | tf_op jit(solution)/shard_map/ppermute | solution.py:243
  44.6 1.4 squeeze.5
  49.7 1.7 %copy.52 = f32[2,384,4]{2,1,0:T(8,128)} copy(f32[2,384,4]{1,2,0:T(4,128)} %param.11) | data formatting | bytes 24576 | tf_op args[4]
  51.3 4.6 %prep.1.r_ref = bf16[12,512,128]{2,1,0:T(8,128)(2,1)} custom-call(bf16[768,256]{1,0:T(8,128)(2,1)} %bitcast.22, bf16[768,256]{1,0:T(8,128)(2,1)} %bitcast.23, f32[768,4]{1,0:T(8,128)} %bitcast.19), custom_call_target="tpu_custom_call" | custom-call | tf_op jit(solution)/shard_map/prep/pallas_call | solution.py:283
  56.0 1.3 fusion.8
  57.3 1.3 collective-permute-start.1
  59.4 3.5 %collective-permute-done.1.refs_0_ = s32[24]{0:T(128)S(1)} collective-permute-done((s32[24]{0:T(128)}, s32[24]{0:T(128)S(1)}, u32[]{:S(2)}, u32[]{:S(2)}) %collective-permute-start.1) | collective-permute-done | bytes 128 | tf_op jit(solution)/shard_map/ppermute | solution.py:243
  63.4 1.8 %pack.1 = (bf16[512,128]{1,0:T(8,128)(2,1)}, bf16[512,128]{1,0:T(8,128)(2,1)}, bf16[512,128]{1,0:T(8,128)(2,1)}) custom-call(s32[24]{0:T(128)} %copy-done.19, s32[24]{0:T(128)} %collective-permute-done.2.refs_1_, s32[24]{0:T(128)} %collective-permute-done.3.refs_2_, bf16[1536,128]{1,0:T(8,128)(2,1)} %maximum_select_fusion.refs_3_.pair_ref), custom_call_target="tpu_custom_call" | custom-call | tf_op jit(solution)/shard_map/pack/pallas_call | solution.py:272
  65.2 3.7 %collective-permute-start.4 = (bf16[512,128]{1,0:T(8,128)(2,1)}, bf16[512,128]{1,0:T(8,128)(2,1)S(1)}, u32[]{:S(2)}, u32[]{:S(2)}) collective-permute-start(bf16[512,128]{1,0:T(8,128)(2,1)} %get-tuple-element.19), channel_id=1, source_target_pairs={{0,8},{4,12},{8,16},{12,20},{16,24},{20,28},{1,9},{5,13},{9,17},{1... | collective-permute-start | bytes 393224 | tf_op jit(solution)/shard_map/ppermute | solution.py:243
  68.9 2.9 %collective-permute-start.5 = (bf16[512,128]{1,0:T(8,128)(2,1)}, bf16[512,128]{1,0:T(8,128)(2,1)S(1)}, u32[]{:S(2)}, u32[]{:S(2)}) collective-permute-start(bf16[512,128]{1,0:T(8,128)(2,1)} %get-tuple-element.20), channel_id=1, source_target_pairs={{0,16},{4,20},{8,24},{12,28},{1,17},{5,21},{9,25},{13,29},{2,18},{... | collective-permute-start | bytes 393224 | tf_op jit(solution)/shard_map/ppermute | solution.py:243
  71.9 1.3 collective-permute-start.6
  74.5 1.5 collective-permute-done.5.refs_1_
  76.0 1.4 collective-permute-done.6.refs_2_
  78.0 21.9 %attend.1 = (bf16[768,256]{1,0:T(8,128)(2,1)}, f32[768,128]{1,0:T(8,128)}, bf16[272,128]{1,0:T(8,128)(2,1)}, bf16[272,128]{1,0:T(8,128)(2,1)}, bf16[272,128]{1,0...) custom-call(s32[192]{0:T(256)} %fusion.6.kv_loc, ...), custom_call_target="tpu_custom_call" | custom-call | tf_op jit(solution)/shard_map/attend/pallas_call | solution.py:323
  101.2 1.3 collective-permute-start.8
  102.5 1.3 collective-permute-start.9
  103.8 2.5 %collective-permute-done.7.refs_0_ = bf16[272,128]{1,0:T(8,128)(2,1)S(1)} collective-permute-done((bf16[272,128]{1,0:T(8,128)(2,1)}, bf16[272,128]{1,0:T(8,128)(2,1)S(1)}, u32[]{:S(2)}, u32[]{:S(2)}) %collective-permute-start.7) | collective-permute-done | bytes 69664 | tf_op jit(solution)/shard_map/ppermute | solution.py:243
  107.6 2.6 %collective-permute-done.8.refs_1_ = bf16[272,128]{1,0:T(8,128)(2,1)S(1)} collective-permute-done((bf16[272,128]{1,0:T(8,128)(2,1)}, bf16[272,128]{1,0:T(8,128)(2,1)S(1)}, u32[]{:S(2)}, u32[]{:S(2)}) %collective-permute-start.8) | collective-permute-done | bytes 69664 | tf_op jit(solution)/shard_map/ppermute | solution.py:243
  111.5 2.5 %collective-permute-done.9.refs_2_ = bf16[272,128]{1,0:T(8,128)(2,1)S(1)} collective-permute-done((bf16[272,128]{1,0:T(8,128)(2,1)}, bf16[272,128]{1,0:T(8,128)(2,1)S(1)}, u32[]{:S(2)}, u32[]{:S(2)}) %collective-permute-start.9) | collective-permute-done | bytes 69664 | tf_op jit(solution)/shard_map/ppermute | solution.py:243
  114.0 1.3 collective-permute-start.12
  115.3 4.9 %collective-permute-done.10.refs_3_ = bf16[272,128]{1,0:T(8,128)(2,1)S(1)} collective-permute-done((bf16[272,128]{1,0:T(8,128)(2,1)}, bf16[272,128]{1,0:T(8,128)(2,1)S(1)}, u32[]{:S(2)}, u32[]{:S(2)}) %collective-permute-start.10) | collective-permute-done | bytes 69664 | tf_op jit(solution)/shard_map/ppermute | solution.py:243
  122.3 7.5 %collective-permute-done.13.refs_6_ = bf16[272,128]{1,0:T(8,128)(2,1)} collective-permute-done((bf16[272,128]{1,0:T(8,128)(2,1)}, bf16[272,128]{1,0:T(8,128)(2,1)}, u32[]{:S(2)}, u32[]{:S(2)}) %collective-permute-start.13) | collective-permute-done | bytes 69664 | tf_op jit(solution)/shard_map/ppermute | solution.py:243
  130.9 5.8 %combine.1 = (bf16[768,64]{1,0:T(8,128)(2,1)}, bf16[768,64]{1,0:T(8,128)(2,1)}, bf16[32,64,128]{2,1,0:T(8,128)(2,1)}) custom-call(s32[1]{0:T(128)} %bitcast.11.quarter, f32[768,128]{1,0:T(8,128)} %get-tuple-element.23.own_ref, bf16[272,128]{1,0:T(8,128)(2,1)} %copy-done.6, bf16[272,128]{1,0:T(8,128)(2,1)} %copy-done.7, bf16[272,128]{1,0:T(8,128)(2,1)} %copy-done.8, ...), custom_call_target="tpu_custom_call" | custom-call | tf_op jit(solution)/shard_map/combine/pallas_call | solution.py:353
  136.7 2.6 %all-to-all-start = ((bf16[32,64,128]{2,1,0:T(8,128)(2,1)}), bf16[32,64,128]{2,1,0:T(8,128)(2,1)S(1)}, u32[]{:S(2)}, u32[]{:S(2)}) async-start(bf16[32,64,128]{2,1,0:T(8,128)(2,1)} %get-tuple-element.33), calls=%async_computation | async-start | bytes 1048576 | tf_op jit(solution)/shard_map/all_to_all | solution.py:370
  139.3 1.7 %copy.57 = bf16[2,384,64]{1,2,0:T(8,128)(2,1)} copy(bf16[2,384,64]{2,1,0:T(8,128)(2,1)} %bitcast.25) | data formatting | bytes 196608
  141.0 1.7 %copy.58 = bf16[2,384,64]{1,2,0:T(8,128)(2,1)} copy(bf16[2,384,64]{2,1,0:T(8,128)(2,1)} %bitcast.24) | data formatting | bytes 196608
  142.7 12.2 %all-to-all-done.in_ref = bf16[32,64,128]{2,1,0:T(8,128)(2,1)S(1)} async-done(((bf16[32,64,128]{2,1,0:T(8,128)(2,1)}), bf16[32,64,128]{2,1,0:T(8,128)(2,1)S(1)}, u32[]{:S(2)}, u32[]{:S(2)}) %all-to-all-start) | async-done | bytes 524320 | tf_op jit(solution)/shard_map/all_to_all | solution.py:370
  155.7 1.8 %final.1 = f32[128,256]{1,0:T(8,128)} custom-call(bf16[32,64,128]{2,1,0:T(8,128)(2,1)} %copy-done), custom_call_target="tpu_custom_call" | custom-call | tf_op jit(solution)/shard_map/final/pallas_call | solution.py:371
  (99 shorter events, 26.9 us)
Async XLA Ops:
  0.6 37.6 %collective-permute-start.15 = (bf16[2,96,4096]{2,1,0:T(8,128)(2,1)}, bf16[2,96,4096]{2,1,0:T(8,128)(2,1)S(1)}, u32[]{:S(2)}, u32[]{:S(2)}) collective-permute-start(bf16[2,96,4096]{2,1,0:T(8,128)(2,1)} %refs_7_.1), channel_id=1, source_target_pairs={{0,2},{1,3},{2,0},{3,1},{4,6},{5,7},{6,4},{7,5},{8,10},{9,11},{10,... | collective-permute-start | bytes 4718600 | tf_op jit(solution)/shard_map/ppermute | solution.py:243
  7.4 52.0 %collective-permute-start.3 = (s32[24]{0:T(128)}, s32[24]{0:T(128)}, u32[]{:S(2)}, u32[]{:S(2)}) collective-permute-start(s32[24]{0:T(128)} %reshape.212), channel_id=1, source_target_pairs={{24,0},{28,4},{25,1},{29,5},{26,2},{30,6},{27,3},{31,7}} | collective-permute-start | bytes 296 | tf_op jit(solution)/shard_map/ppermute | solution.py:243
  8.7 50.7 %collective-permute-start.2 = (s32[24]{0:T(128)}, s32[24]{0:T(128)}, u32[]{:S(2)}, u32[]{:S(2)}) collective-permute-start(s32[24]{0:T(128)} %reshape.212), channel_id=1, source_target_pairs={{16,0},{20,4},{24,8},{28,12},{17,1},{21,5},{25,9},{29,13},{18,2},{... | collective-permute-start | bytes 296 | tf_op jit(solution)/shard_map/ppermute | solution.py:243
  10.0 119.8 %collective-permute-start.14 = (bf16[2,96,4096]{2,1,0:T(8,128)(2,1)}, bf16[2,96,4096]{2,1,0:T(8,128)(2,1)S(1)}, u32[]{:S(2)}, u32[]{:S(2)}) collective-permute-start(bf16[2,96,4096]{2,1,0:T(8,128)(2,1)} %refs_7_.1), channel_id=1, source_target_pairs={{0,1},{1,0},{2,3},{3,2},{4,5},{5,4},{6,7},{7,6},{8,9},{9,8},{10,11... | collective-permute-start | bytes 4718600 | tf_op jit(solution)/shard_map/ppermute | solution.py:243
  11.2 46.0 %collective-permute-start = (bf16[768,128]{1,0:T(8,128)(2,1)S(1)}, bf16[768,128]{1,0:T(8,128)(2,1)S(1)}, u32[]{:S(2)}, u32[]{:S(2)}) collective-permute-start(bf16[768,128]{1,0:T(8,128)(2,1)S(1)} %bitcast.20), channel_id=1, source_target_pairs={{0,4},{4,0},{8,12},{12,8},{16,20},{20,16},{24,28},{28,24},{1,5},{5... | collective-permute-start | bytes 589832 | tf_op jit(solution)/shard_map/ppermute | solution.py:243
  13.6 24.7 %copy-start.15 = (s32[2,6,1]{1,0,2:T(2,128)}, s32[2,6,1]{1,0,2:T(2,128)S(1)}, u32[]{:S(2)}) copy-start(s32[2,6,1]{1,0,2:T(2,128)S(1)} %copy.45) | copy-start | bytes 148
  13.7 24.6 %copy-start.18 = (pred[16]{0:T(512)(128)(4,1)}, pred[16]{0:T(512)(128)(4,1)S(1)}, u32[]{:S(2)}) copy-start(pred[16]{0:T(512)(128)(4,1)S(1)} %iota_compare_fusion) | copy-start | bytes 52
  13.7 26.1 %copy-start.17 = (s32[6]{0:T(128)}, s32[6]{0:T(128)S(1)}, u32[]{:S(2)}) copy-start(s32[6]{0:T(128)S(1)} %iota_add_fusion.1) | copy-start | bytes 76
  38.3 17.7 %copy-start.1 = (bf16[2,96,4096]{2,1,0:T(8,128)(2,1)}, bf16[2,96,4096]{2,1,0:T(8,128)(2,1)S(1)}, u32[]{:S(2)}) copy-start(bf16[2,96,4096]{2,1,0:T(8,128)(2,1)S(1)} %collective-permute-done.15.refs_9_) | copy-start | bytes 4718596
  38.3 91.5 %collective-permute-start.16 = (bf16[2,96,4096]{2,1,0:T(8,128)(2,1)S(1)}, bf16[2,96,4096]{2,1,0:T(8,128)(2,1)}, u32[]{:S(2)}, u32[]{:S(2)}) collective-permute-start(bf16[2,96,4096]{2,1,0:T(8,128)(2,1)S(1)} %collective-permute-done.15.refs_9_), channel_id=1, source_target_pairs={{0,1},{1,0},{2,3},{3,2},{4,5},{5,4},{6,7},{7,6},{8,9},{9,8},{10,11... | collective-permute-start | bytes 4718600 | tf_op jit(solution)/shard_map/ppermute | solution.py:243
  49.7 6.3 %copy-start.13 = (s32[192]{0:T(256)S(1)}, s32[192]{0:T(256)}, u32[]{:S(2)}) copy-start(s32[192]{0:T(256)} %add.185) | copy-start | bytes 2308
  49.7 6.3 %copy-start.14 = (s32[192]{0:T(256)S(1)}, s32[192]{0:T(256)}, u32[]{:S(2)}) copy-start(s32[192]{0:T(256)} %reduce_min.30) | copy-start | bytes 2308
  49.7 6.3 %copy-start.16 = (s32[192]{0:T(256)S(1)}, s32[192]{0:T(256)}, u32[]{:S(2)}) copy-start(s32[192]{0:T(256)} %broadcast_in_dim.93) | copy-start | bytes 2308
  57.3 5.7 %collective-permute-start.1 = (s32[24]{0:T(128)}, s32[24]{0:T(128)S(1)}, u32[]{:S(2)}, u32[]{:S(2)}) collective-permute-start(s32[24]{0:T(128)} %reshape.212), channel_id=1, source_target_pairs={{8,0},{12,4},{16,8},{20,12},{24,16},{28,20},{9,1},{13,5},{17,9},{2... | collective-permute-start | bytes 296 | tf_op jit(solution)/shard_map/ppermute | solution.py:243
  65.2 9.3 %collective-permute-start.4 = (bf16[512,128]{1,0:T(8,128)(2,1)}, bf16[512,128]{1,0:T(8,128)(2,1)S(1)}, u32[]{:S(2)}, u32[]{:S(2)}) collective-permute-start(bf16[512,128]{1,0:T(8,128)(2,1)} %get-tuple-element.19), channel_id=1, source_target_pairs={{0,8},{4,12},{8,16},{12,20},{16,24},{20,28},{1,9},{5,13},{9,17},{1... | collective-permute-start | bytes 393224 | tf_op jit(solution)/shard_map/ppermute | solution.py:243
  68.9 7.0 %collective-permute-start.5 = (bf16[512,128]{1,0:T(8,128)(2,1)}, bf16[512,128]{1,0:T(8,128)(2,1)S(1)}, u32[]{:S(2)}, u32[]{:S(2)}) collective-permute-start(bf16[512,128]{1,0:T(8,128)(2,1)} %get-tuple-element.20), channel_id=1, source_target_pairs={{0,16},{4,20},{8,24},{12,28},{1,17},{5,21},{9,25},{13,29},{2,18},{... | collective-permute-start | bytes 393224 | tf_op jit(solution)/shard_map/ppermute | solution.py:243
  71.9 5.5 %collective-permute-start.6 = (bf16[512,128]{1,0:T(8,128)(2,1)}, bf16[512,128]{1,0:T(8,128)(2,1)S(1)}, u32[]{:S(2)}, u32[]{:S(2)}) collective-permute-start(bf16[512,128]{1,0:T(8,128)(2,1)} %get-tuple-element.21), channel_id=1, source_target_pairs={{0,24},{4,28},{1,25},{5,29},{2,26},{6,30},{3,27},{7,31}} | collective-permute-start | bytes 393224 | tf_op jit(solution)/shard_map/ppermute | solution.py:243
  74.5 2.9 %copy-start.3 = (bf16[512,128]{1,0:T(8,128)(2,1)}, bf16[512,128]{1,0:T(8,128)(2,1)S(1)}, u32[]{:S(2)}) copy-start(bf16[512,128]{1,0:T(8,128)(2,1)S(1)} %collective-permute-done.4.refs_0_) | copy-start | bytes 393220
  76.0 1.4 copy-start.4
  99.9 6.4 %collective-permute-start.7 = (bf16[272,128]{1,0:T(8,128)(2,1)}, bf16[272,128]{1,0:T(8,128)(2,1)S(1)}, u32[]{:S(2)}, u32[]{:S(2)}) collective-permute-start(bf16[272,128]{1,0:T(8,128)(2,1)} %get-tuple-element.24), channel_id=1, source_target_pairs={{4,0},{8,4},{12,8},{16,12},{20,16},{24,20},{28,24},{5,1},{9,5},{13... | collective-permute-start | bytes 208904 | tf_op jit(solution)/shard_map/ppermute | solution.py:243
  101.2 9.0 %collective-permute-start.8 = (bf16[272,128]{1,0:T(8,128)(2,1)}, bf16[272,128]{1,0:T(8,128)(2,1)S(1)}, u32[]{:S(2)}, u32[]{:S(2)}) collective-permute-start(bf16[272,128]{1,0:T(8,128)(2,1)} %get-tuple-element.25), channel_id=1, source_target_pairs={{8,0},{12,4},{16,8},{20,12},{24,16},{28,20},{9,1},{13,5},{17,9},{2... | collective-permute-start | bytes 208904 | tf_op jit(solution)/shard_map/ppermute | solution.py:243
  102.5 11.5 %collective-permute-start.9 = (bf16[272,128]{1,0:T(8,128)(2,1)}, bf16[272,128]{1,0:T(8,128)(2,1)S(1)}, u32[]{:S(2)}, u32[]{:S(2)}) collective-permute-start(bf16[272,128]{1,0:T(8,128)(2,1)} %get-tuple-element.26), channel_id=1, source_target_pairs={{12,0},{16,4},{20,8},{24,12},{28,16},{13,1},{17,5},{21,9},{25,13},... | collective-permute-start | bytes 208904 | tf_op jit(solution)/shard_map/ppermute | solution.py:243
  106.3 23.5 %copy-start.6 = (bf16[272,128]{1,0:T(8,128)(2,1)}, bf16[272,128]{1,0:T(8,128)(2,1)S(1)}, u32[]{:S(2)}) copy-start(bf16[272,128]{1,0:T(8,128)(2,1)S(1)} %collective-permute-done.7.refs_0_) | copy-start | bytes 208900
  106.3 13.8 %collective-permute-start.10 = (bf16[272,128]{1,0:T(8,128)(2,1)}, bf16[272,128]{1,0:T(8,128)(2,1)S(1)}, u32[]{:S(2)}, u32[]{:S(2)}) collective-permute-start(bf16[272,128]{1,0:T(8,128)(2,1)} %get-tuple-element.27), channel_id=1, source_target_pairs={{16,0},{20,4},{24,8},{28,12},{17,1},{21,5},{25,9},{29,13},{18,2},{... | collective-permute-start | bytes 208904 | tf_op jit(solution)/shard_map/ppermute | solution.py:243
  110.2 19.6 %copy-start.7 = (bf16[272,128]{1,0:T(8,128)(2,1)}, bf16[272,128]{1,0:T(8,128)(2,1)S(1)}, u32[]{:S(2)}) copy-start(bf16[272,128]{1,0:T(8,128)(2,1)S(1)} %collective-permute-done.8.refs_1_) | copy-start | bytes 208900
  110.2 11.2 %collective-permute-start.11 = (bf16[272,128]{1,0:T(8,128)(2,1)}, bf16[272,128]{1,0:T(8,128)(2,1)S(1)}, u32[]{:S(2)}, u32[]{:S(2)}) collective-permute-start(bf16[272,128]{1,0:T(8,128)(2,1)} %get-tuple-element.28), channel_id=1, source_target_pairs={{20,0},{24,4},{28,8},{21,1},{25,5},{29,9},{22,2},{26,6},{30,10},{2... | collective-permute-start | bytes 208904 | tf_op jit(solution)/shard_map/ppermute | solution.py:243
  114.0 15.8 %copy-start.8 = (bf16[272,128]{1,0:T(8,128)(2,1)}, bf16[272,128]{1,0:T(8,128)(2,1)S(1)}, u32[]{:S(2)}) copy-start(bf16[272,128]{1,0:T(8,128)(2,1)S(1)} %collective-permute-done.9.refs_2_) | copy-start | bytes 208900
  114.0 8.3 %collective-permute-start.12 = (bf16[272,128]{1,0:T(8,128)(2,1)}, bf16[272,128]{1,0:T(8,128)(2,1)}, u32[]{:S(2)}, u32[]{:S(2)}) collective-permute-start(bf16[272,128]{1,0:T(8,128)(2,1)} %get-tuple-element.29), channel_id=1, source_target_pairs={{24,0},{28,4},{25,1},{29,5},{26,2},{30,6},{27,3},{31,7}} | collective-permute-start | bytes 208904 | tf_op jit(solution)/shard_map/ppermute | solution.py:243
  120.1 9.7 %copy-start.9 = (bf16[272,128]{1,0:T(8,128)(2,1)}, bf16[272,128]{1,0:T(8,128)(2,1)S(1)}, u32[]{:S(2)}) copy-start(bf16[272,128]{1,0:T(8,128)(2,1)S(1)} %collective-permute-done.10.refs_3_) | copy-start | bytes 208900
  120.1 9.6 %collective-permute-start.13 = (bf16[272,128]{1,0:T(8,128)(2,1)}, bf16[272,128]{1,0:T(8,128)(2,1)}, u32[]{:S(2)}, u32[]{:S(2)}) collective-permute-start(bf16[272,128]{1,0:T(8,128)(2,1)} %get-tuple-element.30), channel_id=1, source_target_pairs={{28,0},{29,1},{30,2},{31,3}} | collective-permute-start | bytes 208904 | tf_op jit(solution)/shard_map/ppermute | solution.py:243
  121.5 8.4 %copy-start.10 = (bf16[272,128]{1,0:T(8,128)(2,1)}, bf16[272,128]{1,0:T(8,128)(2,1)S(1)}, u32[]{:S(2)}) copy-start(bf16[272,128]{1,0:T(8,128)(2,1)S(1)} %collective-permute-done.11.refs_4_) | copy-start | bytes 208900
  136.7 18.2 %all-to-all-start = ((bf16[32,64,128]{2,1,0:T(8,128)(2,1)}), bf16[32,64,128]{2,1,0:T(8,128)(2,1)S(1)}, u32[]{:S(2)}, u32[]{:S(2)}) async-start(bf16[32,64,128]{2,1,0:T(8,128)(2,1)} %get-tuple-element.33), calls=%async_computation | async-start | bytes 1048576 | tf_op jit(solution)/shard_map/all_to_all | solution.py:370
  (6 other events, 4.3 us)
